TPU v7x, 32 devices: a whole 2x2x4 slice. The times are simulated.
32 devices in a mesh: rep: 2 (over x), fs: 8 (over z, y), tp: 2 (over core).
Axes of the slice: x: 2, y: 2, z: 4, core: 2. Of those that a mesh axis runs over, the one named last changes fastest.
Arguments:
- tokens: bfloat16 [4096, 2048], P(('rep', 'fs', 'tp')), may hold values from -6 to 6
- mix_gain: float32 [2048], replicated, may hold values from 0.1 to 1.9
- conv_in_weight: bfloat16 [2048, 1024], P('fs', 'tp'), may hold values from -0.125 to 0.125
- gate_outer_weight: bfloat16 [2048, 1024], P('fs', 'tp'), may hold values from -0.125 to 0.125
- gate_inner_weight: bfloat16 [2048, 1024], P('fs', 'tp'), may hold values from -0.125 to 0.125
- conv_taps: float32 [3, 1024], P(None, 'tp'), may hold values from -3.5 to 3.5
- out_weight: bfloat16 [1024, 2048], P('tp', 'fs'), may hold values from -0.1875 to 0.1875
- ff_gain: float32 [2048], replicated, may hold values from 0.1 to 1.9
- up_weight: bfloat16 [2048, 8192], P('fs', 'tp'), may hold values from -0.125 to 0.125
- down_weight: bfloat16 [8192, 2048], P('tp', 'fs'), may hold values from -0.0625 to 0.0625
Outputs:
- layer_out: bfloat16 [4096, 2048], P(('rep', 'fs', 'tp'))
All inputs are finite; a program needn't handle non-finite values.
Results may differ from a plain program's by a relative error of at most 0.023.
Values may be sent and summed in bfloat16 or wider, within the bound.
A program may use at most 128 MiB of HBM per device.

v0:
```python
import jax
import jax.numpy as jnp
from jax import lax
from jax.sharding import PartitionSpec as P

eps = 1e-06


def rms_scale(values, gain):
    widened = values.astype(jnp.float32)
    inverse = lax.rsqrt(jnp.mean(widened * widened, axis=-1, keepdims=True) + eps)
    return (widened * inverse * gain).astype(jnp.bfloat16)


def on_device(
    tokens,
    mix_gain,
    conv_in_weight,
    gate_outer_weight,
    gate_inner_weight,
    conv_taps,
    out_weight,
    ff_gain,
    up_weight,
    down_weight,
):
    normed = rms_scale(tokens, mix_gain)
    gathered = lax.all_gather(normed, "tp", axis=0, tiled=True)
    seq_rows = gathered.shape[0]
    segment = (
        lax.all_gather(conv_in_weight, "fs", axis=0, tiled=True),
        lax.all_gather(gate_outer_weight, "fs", axis=0, tiled=True),
        lax.all_gather(gate_inner_weight, "fs", axis=0, tiled=True),
    )
    conv_input, gate_outer, gate_inner = tuple(
        (jnp.dot(gathered, weight, preferred_element_type=jnp.float32) for weight in segment)
    )
    conv_input = conv_input.astype(jnp.bfloat16)
    gate_outer = gate_outer.astype(jnp.bfloat16)
    gate_inner = gate_inner.astype(jnp.bfloat16)
    gated = gate_inner.astype(jnp.float32) * conv_input.astype(jnp.float32)
    padded = jnp.pad(gated, ((2, 0), (0, 0)))
    convolved = (
        conv_taps[0] * padded[0:seq_rows]
        + conv_taps[1] * padded[1 : seq_rows + 1]
        + conv_taps[2] * padded[2 : seq_rows + 2]
    )
    mixed = (gate_outer.astype(jnp.float32) * convolved).astype(jnp.bfloat16)
    out_full = lax.all_gather(out_weight, "fs", axis=1, tiled=True)
    lefts = mixed
    mix_total = lax.psum_scatter(
        jnp.dot(lefts, out_full, preferred_element_type=jnp.float32).astype(jnp.bfloat16),
        "tp",
        scatter_dimension=0,
        tiled=True,
    ).astype(jnp.float32)
    resid = (tokens.astype(jnp.float32) + mix_total).astype(jnp.bfloat16)
    normed_ff = rms_scale(resid, ff_gain)
    ff_gathered = lax.all_gather(normed_ff, "tp", axis=0, tiled=True)
    up_full = lax.all_gather(up_weight, "fs", axis=0, tiled=True)
    preact = jnp.dot(ff_gathered, up_full, preferred_element_type=jnp.float32)
    hidden = jnp.square(jax.nn.relu(preact)).astype(jnp.bfloat16)
    down_full = lax.all_gather(down_weight, "fs", axis=1, tiled=True)
    lefts = hidden
    ff_total = lax.psum_scatter(
        jnp.dot(lefts, down_full, preferred_element_type=jnp.float32).astype(jnp.bfloat16),
        "tp",
        scatter_dimension=0,
        tiled=True,
    ).astype(jnp.float32)
    return (resid.astype(jnp.float32) + ff_total).astype(jnp.bfloat16)


def solution(mesh):
    in_specs = (
        P(("rep", "fs", "tp"), None),
        P(),
        P("fs", "tp"),
        P("fs", "tp"),
        P("fs", "tp"),
        P(None, "tp"),
        P("tp", "fs"),
        P(),
        P("fs", "tp"),
        P("tp", "fs"),
    )
    out_specs = P(("rep", "fs", "tp"), None)
    return jax.shard_map(
        on_device, mesh=mesh, in_specs=in_specs, out_specs=out_specs, check_vma=False
    )
```

profile of v0, /device:TPU:0, one launch (start us, length us, event | category | flops | bytes accessed | tf_op | source)
XLA Modules:
  0.0 740.0 jit_solution(13610082769893983982)
XLA Ops:
  6.5 0.0 copy-start.4
  6.5 0.0 all-gather.9.cloned.1.call-start
  6.5 1.2 fusion.8
  7.8 2.0 fusion.10
  9.8 0.0 all-gather.9.cloned.1.call-update
  9.8 0.0 all-gather.15.cloned.1.call-start
  9.9 0.7 all-gather.15.cloned.1.call-update
  10.6 0.0 all-gather.13.cloned.1.call-start
  10.6 0.7 all-gather.13.cloned.1.call-update
  11.3 0.0 all-gather.11.cloned.1.call-start
  11.4 0.5 all-gather.11.cloned.1.call-update
  11.9 0.0 all-gather.17.cloned.1.call-start
  12.0 0.5 all-gather.17.cloned.1.call-update
  12.5 0.0 reduce-scatter.3.cloned.1.call-start
  12.5 0.0 copy-done.4
  12.6 9.2 %all-gather.9.cloned.1.call-done = bf16[256,2048]{1,0:T(8,128)(2,1)} async-done(((bf16[128,2048]{1,0:T(8,128)(2,1)}), bf16[256,2048]{1,0:T(8,128)(2,1)}) %all-gather.9.cloned.1.call-update) | async-done | bytes 1048592 | tf_op jit(solution)/shard_map/all_gather | solution.py:28
  21.7 0.0 copy-start.2
  21.7 52.4 %all-gather.15.cloned.1.call-done = bf16[2048,512]{1,0:T(8,128)(2,1)} async-done(((bf16[256,512]{1,0:T(8,128)(2,1)}), bf16[2048,512]{1,0:T(8,128)(2,1)}) %all-gather.15.cloned.1.call-update) | async-done | bytes 2097168 | tf_op jit(solution)/shard_map/all_gather | solution.py:31
  74.2 2.6 fusion.7
  76.8 47.2 %all-gather.13.cloned.1.call-done = bf16[2048,512]{1,0:T(8,128)(2,1)} async-done(((bf16[256,512]{1,0:T(8,128)(2,1)}), bf16[2048,512]{1,0:T(8,128)(2,1)}) %all-gather.13.cloned.1.call-update) | async-done | bytes 2097168 | tf_op jit(solution)/shard_map/all_gather | solution.py:33
  123.9 0.0 copy-done.2
  124.0 2.3 fusion.6
  126.3 47.3 %all-gather.11.cloned.1.call-done = bf16[2048,512]{1,0:T(8,128)(2,1)} async-done(((bf16[256,512]{1,0:T(8,128)(2,1)}), bf16[2048,512]{1,0:T(8,128)(2,1)}) %all-gather.11.cloned.1.call-update) | async-done | bytes 2097168 | tf_op jit(solution)/shard_map/all_gather | solution.py:32
  173.6 50.8 %all-gather.17.cloned.1.call-done = bf16[512,2048]{1,0:T(8,128)(2,1)} async-done(((bf16[512,256]{1,0:T(8,128)(2,1)}), bf16[512,2048]{1,0:T(8,128)(2,1)}) %all-gather.17.cloned.1.call-update) | async-done | bytes 2097168 | tf_op jit(solution)/shard_map/all_gather | solution.py:49
  224.4 0.0 copy-start
  224.4 4.7 convolution_convert_fusion.1
  229.1 0.0 copy-start.3
  229.1 0.0 reduce-scatter.3.cloned.1.call-update
  229.1 0.0 all-gather.19.cloned.1.call-start
  229.2 6.7 reduce-scatter.3.cloned.1.call-done
  235.8 0.0 copy-done
  235.9 1.3 fusion.12
  237.2 0.0 copy-done.3
  237.2 2.0 fusion.14
  239.2 0.0 all-gather.19.cloned.1.call-update
  239.2 0.0 all-gather.21.cloned.1.call-start
  239.3 0.7 all-gather.21.cloned.1.call-update
  240.0 0.0 all-gather.23.cloned.1.call-start
  240.0 0.7 all-gather.23.cloned.1.call-update
  240.7 0.0 copy-start.1
  240.7 0.0 reduce-scatter.5.cloned.1.call-start
  240.8 8.9 %all-gather.19.cloned.1.call-done = bf16[256,2048]{1,0:T(8,128)(2,1)} async-done(((bf16[128,2048]{1,0:T(8,128)(2,1)}), bf16[256,2048]{1,0:T(8,128)(2,1)}) %all-gather.19.cloned.1.call-update) | async-done | bytes 1048592 | tf_op jit(solution)/shard_map/all_gather | solution.py:59
  249.6 230.6 %all-gather.21.cloned.1.call-done = bf16[2048,4096]{1,0:T(8,128)(2,1)} async-done(((bf16[256,4096]{1,0:T(8,128)(2,1)}), bf16[2048,4096]{1,0:T(8,128)(2,1)}) %all-gather.21.cloned.1.call-update) | async-done | bytes 16777232 | tf_op jit(solution)/shard_map/all_gather | solution.py:60
  480.2 227.6 %all-gather.23.cloned.1.call-done = bf16[4096,2048]{1,0:T(8,128)(2,1)} async-done(((bf16[4096,256]{1,0:T(8,128)(2,1)}), bf16[4096,2048]{1,0:T(8,128)(2,1)}) %all-gather.23.cloned.1.call-update) | async-done | bytes 16777232 | tf_op jit(solution)/shard_map/all_gather | solution.py:63
  707.8 16.5 %convolution_convert_fusion = bf16[256,2048]{1,0:T(8,128)(2,1)} fusion(bf16[4096,2048]{1,0:T(8,128)(2,1)} %all-gather.23.cloned.1.call-done, bf16[256,2048]{1,0:T(8,128)(2,1)} %all-gather.19.cloned.1.call-done, bf16[2048,4096]{1,0:T(8,128)(2,1)} %all-gather.21.cloned.1.call-done), kind=kOutput, calls=%fused_computation.3 | convolution fusion | flops 8593604608 | bytes 35651584 | tf_op jit(solution)/shard_map/dot_general | solution.py:66
  724.3 0.0 reduce-scatter.5.cloned.1.call-update
  724.4 6.7 reduce-scatter.5.cloned.1.call-done
  731.1 0.0 copy-done.1
  731.1 2.1 fusion.15
  (3 shorter events, 0.0 us)
Async XLA Ops:
  6.5 6.0 copy-start.4
  6.5 15.2 %all-gather.9.cloned.1.call-start = ((), (), s32[]{:S(2)}) async-start(), calls=%async_computation.2 | async-start | bytes 1572864 | tf_op jit(solution)/shard_map/all_gather | solution.py:28
  9.8 64.3 %all-gather.15.cloned.1.call-start = ((), (), s32[]{:S(2)}) async-start(), calls=%async_computation.5 | async-start | bytes 2359296 | tf_op jit(solution)/shard_map/all_gather | solution.py:31
  10.6 113.4 %all-gather.13.cloned.1.call-start = ((), (), s32[]{:S(2)}) async-start(), calls=%async_computation.4 | async-start | bytes 2359296 | tf_op jit(solution)/shard_map/all_gather | solution.py:33
  11.3 162.3 %all-gather.11.cloned.1.call-start = ((), (), s32[]{:S(2)}) async-start(), calls=%async_computation.3 | async-start | bytes 2359296 | tf_op jit(solution)/shard_map/all_gather | solution.py:32
  11.9 212.5 %all-gather.17.cloned.1.call-start = ((), (), s32[]{:S(2)}) async-start(), calls=%async_computation.6 | async-start | bytes 2359296 | tf_op jit(solution)/shard_map/all_gather | solution.py:49
  12.5 223.4 %reduce-scatter.3.cloned.1.call-start = ((), (), s32[]{:S(2)}) async-start(), calls=%async_computation.7 | async-start | bytes 1572864 | tf_op jit(solution)/shard_map/reduce_scatter | solution.py:51
  21.7 102.2 %copy-start.2 = (bf16[256,2048]{1,0:T(8,128)(2,1)S(1)}, bf16[256,2048]{1,0:T(8,128)(2,1)}, u32[]{:S(2)}) copy-start(bf16[256,2048]{1,0:T(8,128)(2,1)} %all-gather.9.cloned.1.call-done) | copy-start | bytes 3145732
  224.4 11.5 %copy-start = (bf16[128,2048]{1,0:T(8,128)(2,1)S(1)}, bf16[128,2048]{1,0:T(8,128)(2,1)}, u32[]{:S(2)}) copy-start(bf16[128,2048]{1,0:T(8,128)(2,1)} %param.10) | copy-start | bytes 1572868
  229.1 8.1 %copy-start.3 = (f32[2048]{0:T(1024)S(1)}, f32[2048]{0:T(1024)}, u32[]{:S(2)}) copy-start(f32[2048]{0:T(1024)} %param.17) | copy-start | bytes 24580
  229.1 20.5 %all-gather.19.cloned.1.call-start = ((), (), s32[]{:S(2)}) async-start(), calls=%async_computation.8 | async-start | bytes 1572864 | tf_op jit(solution)/shard_map/all_gather | solution.py:59
  239.2 241.0 %all-gather.21.cloned.1.call-start = ((), (), s32[]{:S(2)}) async-start(), calls=%async_computation.9 | async-start | bytes 18874368 | tf_op jit(solution)/shard_map/all_gather | solution.py:60
  240.0 467.8 %all-gather.23.cloned.1.call-start = ((), (), s32[]{:S(2)}) async-start(), calls=%async_computation.10 | async-start | bytes 18874368 | tf_op jit(solution)/shard_map/all_gather | solution.py:63
  240.7 490.4 %copy-start.1 = (bf16[128,2048]{1,0:T(8,128)(2,1)S(1)}, bf16[128,2048]{1,0:T(8,128)(2,1)}, u32[]{:S(2)}) copy-start(bf16[128,2048]{1,0:T(8,128)(2,1)} %reduce-scatter.3.cloned.1.call-done) | copy-start | bytes 1572868
  240.7 490.4 %reduce-scatter.5.cloned.1.call-start = ((), (), s32[]{:S(2)}) async-start(), calls=%async_computation.11 | async-start | bytes 1572864 | tf_op jit(solution)/shard_map/reduce_scatter | solution.py:65
Sparse Core Ops, SparseCore 0:
  10.0 11.7 all-gather.8
  23.9 50.2 all-gather.14
  76.3 47.6 all-gather.12
  125.9 47.6 all-gather.10
  175.5 48.8 all-gather.16
  229.2 6.5 reduce-scatter.2
  239.3 10.2 all-gather.18
  251.7 228.4 all-gather.20
  482.3 225.4 all-gather.22
  724.5 6.5 reduce-scatter.4
where the time goes:
time: 740 us
  waiting for transfers between devices  691 us (93%)
  matrix products  26.2 us (4%)
  between operations  13.6 us (2%)
  other arithmetic  8.69 us (1%)
    all_gather x1, waiting for transfers between devices, on_device(): up_full = lax.all_gather(up_weight, 'fs', axis=0, tiled=True)  231 us
    all_gather x1, waiting for transfers between devices, on_device(): down_full = lax.all_gather(down_weight, 'fs', axis=1, tiled=True)  228 us
    all_gather x1, waiting for transfers between devices, on_device(): lax.all_gather(conv_in_weight, 'fs', axis=0, tiled=True)  52.4 us
    all_gather x1, waiting for transfers between devices, on_device(): out_full = lax.all_gather(out_weight, 'fs', axis=1, tiled=True)  50.8 us
    all_gather x1, waiting for transfers between devices, on_device(): lax.all_gather(gate_outer_weight, 'fs', axis=0, tiled=True)  47.3 us
    all_gather x1, waiting for transfers between devices, on_device(): lax.all_gather(gate_inner_weight, 'fs', axis=0, tiled=True)  47.2 us
    dot_general x1, matrix products, on_device(): jnp.dot(lefts, down_full, preferred_element_type=jnp.float32)  16.5 us
  transfers between devices with their start and end apart: 10, of which 10 were waited for; matrix products, arithmetic and copies ran while one was open for 1% of the time, Pallas kernels for 0%

commit v1 on v0

--- a/solution.py
+++ b/solution.py
@@ -60,7 +60,12 @@
     up_full = lax.all_gather(up_weight, "fs", axis=0, tiled=True)
     preact = jnp.dot(ff_gathered, up_full, preferred_element_type=jnp.float32)
     hidden = jnp.square(jax.nn.relu(preact)).astype(jnp.bfloat16)
-    down_full = lax.all_gather(down_weight, "fs", axis=1, tiled=True)
+    ring = [down_weight]
+    for hop in range(7):
+        ring.append(lax.ppermute(ring[-1], "fs", [(dev, (dev + 1) % 8) for dev in range(8)]))
+    down_full = jnp.roll(
+        jnp.concatenate(ring[::-1], axis=1), (lax.axis_index("fs") + 1) * ring[0].shape[1], axis=1
+    )
     lefts = hidden
     ff_total = lax.psum_scatter(
         jnp.dot(lefts, down_full, preferred_element_type=jnp.float32).astype(jnp.bfloat16),

time: 740 us -> 842 us (1.14)
  waiting for transfers between devices: 691 us -> 748 us
  local copies, waits for them, and re-layouts: 0.03 us -> 41.2 us
    ppermute x0 -> x7, waiting for transfers between devices: none -> 527 us  [on_device(): lax.ppermute(ring[-1], 'fs', [(dev, (dev + 1) % 8) for dev in range(8)])]
    all_gather x1, waiting for transfers between devices: 231 us -> 0.01 us  [on_device(): up_full = lax.all_gather(up_weight, 'fs', axis=0, tiled=True)]
    all_gather x1 -> x0, waiting for transfers between devices: 228 us -> none  [on_device(): down_full = lax.all_gather(down_weight, 'fs', axis=1, tiled=True)]
    unnamed x10 -> x43, local copies, waits for them, and re-layouts: 0.02 us -> 38.9 us
    all_gather x1, waiting for transfers between devices: 8.85 us -> 0.01 us  [on_device(): ff_gathered = lax.all_gather(normed_ff, 'tp', axis=0, tiled=True)]
  transfers between devices with their start and end apart: 10 -> 16, of which waited for: 10 -> 14; matrix products, arithmetic and copies ran while one was open for 1% -> 5% of each run, Pallas kernels for 0% -> 0%
where the time goes in v1:
time: 842 us; the launch traced here: 841 us
  waiting for transfers between devices  748 us (89%)
  local copies, waits for them, and re-layouts  41.2 us (5%)
  matrix products  27.6 us (3%)
  between operations  13.3 us (2%)
  other arithmetic  8.84 us (1%)
    ppermute x7, waiting for transfers between devices, on_device(): lax.ppermute(ring[-1], 'fs', [(dev, (dev + 1) % 8) for dev in range(8)])  527 us
    all_gather x1, waiting for transfers between devices, on_device(): lax.all_gather(conv_in_weight, 'fs', axis=0, tiled=True)  52.4 us
    all_gather x1, waiting for transfers between devices, on_device(): out_full = lax.all_gather(out_weight, 'fs', axis=1, tiled=True)  50.8 us
    all_gather x1, waiting for transfers between devices, on_device(): lax.all_gather(gate_outer_weight, 'fs', axis=0, tiled=True)  46.9 us
    all_gather x1, waiting for transfers between devices, on_device(): lax.all_gather(gate_inner_weight, 'fs', axis=0, tiled=True)  46.4 us
    unnamed x43, local copies, waits for them, and re-layouts  38.9 us
  transfers between devices with their start and end apart: 16, of which 14 were waited for; matrix products, arithmetic and copies ran while one was open for 5% of the time, Pallas kernels for 0%

profile of v1, /device:TPU:0, one launch (start us, length us, event | category | flops | bytes accessed | tf_op | source)
XLA Modules:
  0.0 841.3 jit_solution(695198513787674951)
XLA Ops:
  6.5 1.4 fusion.13
  7.9 2.0 fusion.15
  10.0 0.0 all-gather.8.cloned.1.call-update
  10.0 0.0 all-gather.14.cloned.1.call-start
  10.0 0.7 all-gather.14.cloned.1.call-update
  10.7 0.0 all-gather.12.cloned.1.call-start
  10.8 0.7 all-gather.12.cloned.1.call-update
  11.5 0.0 all-gather.10.cloned.1.call-start
  11.5 0.5 all-gather.10.cloned.1.call-update
  12.0 0.0 all-gather.16.cloned.1.call-start
  12.1 0.5 all-gather.16.cloned.1.call-update
  12.6 0.0 reduce-scatter.3.cloned.1.call-start
  12.7 0.8 fusion.35
  13.5 8.4 all-gather.8.cloned.1.call-done
  21.9 52.4 %all-gather.14.cloned.1.call-done = bf16[2048,512]{1,0:T(8,128)(2,1)} async-done(((bf16[256,512]{1,0:T(8,128)(2,1)}), bf16[2048,512]{1,0:T(8,128)(2,1)}) %all-gather.14.cloned.1.call-update) | async-done | bytes 2097168 | tf_op jit(solution)/shard_map/all_gather | solution.py:31
  74.3 3.4 fusion.12
  77.7 46.4 %all-gather.12.cloned.1.call-done = bf16[2048,512]{1,0:T(8,128)(2,1)} async-done(((bf16[256,512]{1,0:T(8,128)(2,1)}), bf16[2048,512]{1,0:T(8,128)(2,1)}) %all-gather.12.cloned.1.call-update) | async-done | bytes 2097168 | tf_op jit(solution)/shard_map/all_gather | solution.py:33
  124.1 2.7 fusion.11
  126.8 46.9 %all-gather.10.cloned.1.call-done = bf16[2048,512]{1,0:T(8,128)(2,1)} async-done(((bf16[256,512]{1,0:T(8,128)(2,1)}), bf16[2048,512]{1,0:T(8,128)(2,1)}) %all-gather.10.cloned.1.call-update) | async-done | bytes 2097168 | tf_op jit(solution)/shard_map/all_gather | solution.py:32
  173.7 50.8 %all-gather.16.cloned.1.call-done = bf16[512,2048]{1,0:T(8,128)(2,1)} async-done(((bf16[512,256]{1,0:T(8,128)(2,1)}), bf16[512,2048]{1,0:T(8,128)(2,1)}) %all-gather.16.cloned.1.call-update) | async-done | bytes 2097168 | tf_op jit(solution)/shard_map/all_gather | solution.py:49
  224.5 5.0 convolution_convert_fusion
  229.5 0.0 reduce-scatter.3.cloned.1.call-update
  229.5 0.0 all-gather.18.cloned.1.call-start
  229.6 6.7 reduce-scatter.3.cloned.1.call-done
  236.2 1.3 fusion.17
  237.5 2.0 fusion.19
  239.6 0.0 all-gather.18.cloned.1.call-update
  239.6 0.0 all-gather.20.cloned.1.call-start
  239.7 0.7 all-gather.20.cloned.1.call-update
  240.4 0.0 reduce-scatter.5.cloned.1.call-start
  240.4 1.8 collective-permute-start
  242.3 71.6 %collective-permute-done = bf16[4096,256]{1,0:T(8,128)(2,1)S(1)} collective-permute-done((bf16[4096,256]{1,0:T(8,128)(2,1)S(1)}, bf16[4096,256]{1,0:T(8,128)(2,1)S(1)}, u32[]{:S(2)}, u32[]{:S(2)}) %collective-permute-start) | collective-permute-done | bytes 2097184 | tf_op jit(solution)/shard_map/ppermute | solution.py:65
  313.9 1.4 copy-done.2
  315.2 0.0 collective-permute-start.1
  315.2 88.4 %collective-permute-done.1 = bf16[4096,256]{1,0:T(8,128)(2,1)S(1)} collective-permute-done((bf16[4096,256]{1,0:T(8,128)(2,1)S(1)}, bf16[4096,256]{1,0:T(8,128)(2,1)S(1)}, u32[]{:S(2)}, u32[]{:S(2)}) %collective-permute-start.1) | collective-permute-done | bytes 2097184 | tf_op jit(solution)/shard_map/ppermute | solution.py:65
  403.6 1.3 copy-done.4
  405.0 95.6 %collective-permute-done.2 = bf16[4096,256]{1,0:T(8,128)(2,1)S(1)} collective-permute-done((bf16[4096,256]{1,0:T(8,128)(2,1)S(1)}, bf16[4096,256]{1,0:T(8,128)(2,1)S(1)}, u32[]{:S(2)}, u32[]{:S(2)}) %collective-permute-start.2) | collective-permute-done | bytes 2097184 | tf_op jit(solution)/shard_map/ppermute | solution.py:65
  500.5 1.3 copy-done.6
  501.9 95.3 %collective-permute-done.3 = bf16[4096,256]{1,0:T(8,128)(2,1)S(1)} collective-permute-done((bf16[4096,256]{1,0:T(8,128)(2,1)S(1)}, bf16[4096,256]{1,0:T(8,128)(2,1)S(1)}, u32[]{:S(2)}, u32[]{:S(2)}) %collective-permute-start.3) | collective-permute-done | bytes 2097184 | tf_op jit(solution)/shard_map/ppermute | solution.py:65
  597.2 1.3 copy-done.8
  598.5 76.4 %collective-permute-done.4 = bf16[4096,256]{1,0:T(8,128)(2,1)S(1)} collective-permute-done((bf16[4096,256]{1,0:T(8,128)(2,1)S(1)}, bf16[4096,256]{1,0:T(8,128)(2,1)S(1)}, u32[]{:S(2)}, u32[]{:S(2)}) %collective-permute-start.4) | collective-permute-done | bytes 2097184 | tf_op jit(solution)/shard_map/ppermute | solution.py:65
  675.0 1.3 copy-done.10
  676.3 50.5 %collective-permute-done.5 = bf16[4096,256]{1,0:T(8,128)(2,1)} collective-permute-done((bf16[4096,256]{1,0:T(8,128)(2,1)S(1)}, bf16[4096,256]{1,0:T(8,128)(2,1)}, u32[]{:S(2)}, u32[]{:S(2)}) %collective-permute-start.5) | collective-permute-done | bytes 2097184 | tf_op jit(solution)/shard_map/ppermute | solution.py:65
  726.8 49.2 %collective-permute-done.6 = bf16[4096,256]{1,0:T(8,128)(2,1)} collective-permute-done((bf16[4096,256]{1,0:T(8,128)(2,1)}, bf16[4096,256]{1,0:T(8,128)(2,1)}, u32[]{:S(2)}, u32[]{:S(2)}) %collective-permute-start.6) | collective-permute-done | bytes 2097184 | tf_op jit(solution)/shard_map/ppermute | solution.py:65
  776.0 3.1 constant_dynamic-update-slice_fusion.15
  779.0 3.1 constant_dynamic-update-slice_fusion.14
  782.1 3.2 constant_dynamic-update-slice_fusion.13
  785.3 3.2 constant_dynamic-update-slice_fusion.12
  788.6 1.5 constant_dynamic-update-slice_fusion.11
  790.1 1.5 constant_dynamic-update-slice_fusion.10
  791.5 1.5 constant_dynamic-update-slice_fusion.9
  793.0 1.6 constant_dynamic-update-slice_fusion.8
  794.6 3.1 constant_dynamic-update-slice_fusion.7
  797.7 3.1 constant_dynamic-update-slice_fusion.6
  800.8 1.5 constant_dynamic-update-slice_fusion.5
  802.3 1.5 constant_dynamic-update-slice_fusion.4
  803.8 1.5 constant_dynamic-update-slice_fusion.3
  805.3 1.5 constant_dynamic-update-slice_fusion.2
  806.7 1.5 constant_dynamic-update-slice_fusion.1
  808.2 1.5 constant_dynamic-update-slice_fusion
  809.7 16.5 %fusion.4 = bf16[256,2048]{1,0:T(8,128)(2,1)} fusion(bf16[4096,4096]{1,0:T(8,128)(2,1)} %constant_dynamic-update-slice_fusion, s32[]{:T(128)S(6)} %select_n.14, bf16[256,2048]{1,0:T(8,128)(2,1)} %all-gather.18.cloned.1.call-done, bf16[2048,4096]{1,0:T(8,128)(2,1)} %all-gather.20.cloned.1.call-done), kind=kOutput, calls=%fused_computation.6 | convolution fusion | flops 8593604608 | bytes 35651588 | tf_op jit(solution)/shard_map/dot_general | solution.py:71
  826.2 0.0 reduce-scatter.5.cloned.1.call-update
  826.3 6.4 reduce-scatter.5.cloned.1.call-done
  832.6 2.1 fusion.20
  (33 shorter events, 0.1 us)
Async XLA Ops:
  6.5 229.7 %copy-start = (bf16[128,2048]{1,0:T(8,128)(2,1)S(1)}, bf16[128,2048]{1,0:T(8,128)(2,1)}, u32[]{:S(2)}) copy-start(bf16[128,2048]{1,0:T(8,128)(2,1)} %param.10) | copy-start | bytes 1572868
  6.5 231.0 %copy-start.13 = (f32[2048]{0:T(1024)S(1)}, f32[2048]{0:T(1024)}, u32[]{:S(2)}) copy-start(f32[2048]{0:T(1024)} %param.17) | copy-start | bytes 24580
  6.5 233.9 %copy-start.1 = (bf16[4096,256]{1,0:T(8,128)(2,1)S(1)}, bf16[4096,256]{1,0:T(8,128)(2,1)}, u32[]{:S(2)}) copy-start(bf16[4096,256]{1,0:T(8,128)(2,1)} %param.19) | copy-start | bytes 6291460
  6.5 15.3 %all-gather.8.cloned.1.call-start = ((), (), s32[]{:S(2)}) async-start(), calls=%async_computation.2 | async-start | bytes 1572864 | tf_op jit(solution)/shard_map/all_gather | solution.py:28
  10.0 64.3 %all-gather.14.cloned.1.call-start = ((), (), s32[]{:S(2)}) async-start(), calls=%async_computation.5 | async-start | bytes 2359296 | tf_op jit(solution)/shard_map/all_gather | solution.py:31
  10.7 113.4 %all-gather.12.cloned.1.call-start = ((), (), s32[]{:S(2)}) async-start(), calls=%async_computation.4 | async-start | bytes 2359296 | tf_op jit(solution)/shard_map/all_gather | solution.py:33
  11.5 162.3 %all-gather.10.cloned.1.call-start = ((), (), s32[]{:S(2)}) async-start(), calls=%async_computation.3 | async-start | bytes 2359296 | tf_op jit(solution)/shard_map/all_gather | solution.py:32
  12.0 212.5 %all-gather.16.cloned.1.call-start = ((), (), s32[]{:S(2)}) async-start(), calls=%async_computation.6 | async-start | bytes 2359296 | tf_op jit(solution)/shard_map/all_gather | solution.py:49
  12.6 223.6 %reduce-scatter.3.cloned.1.call-start = ((), (), s32[]{:S(2)}) async-start(), calls=%async_computation.7 | async-start | bytes 1572864 | tf_op jit(solution)/shard_map/reduce_scatter | solution.py:51
  229.5 580.2 %all-gather.18.cloned.1.call-start = ((), (), s32[]{:S(2)}) async-start(), calls=%async_computation.8 | async-start | bytes 1572864 | tf_op jit(solution)/shard_map/all_gather | solution.py:59
  239.6 570.1 %all-gather.20.cloned.1.call-start = ((), (), s32[]{:S(2)}) async-start(), calls=%async_computation.9 | async-start | bytes 18874368 | tf_op jit(solution)/shard_map/all_gather | solution.py:60
  240.4 592.3 %reduce-scatter.5.cloned.1.call-start = ((), (), s32[]{:S(2)}) async-start(), calls=%async_computation.10 | async-start | bytes 1572864 | tf_op jit(solution)/shard_map/reduce_scatter | solution.py:70
  240.4 73.4 %collective-permute-start = (bf16[4096,256]{1,0:T(8,128)(2,1)S(1)}, bf16[4096,256]{1,0:T(8,128)(2,1)S(1)}, u32[]{:S(2)}, u32[]{:S(2)}) collective-permute-start(bf16[4096,256]{1,0:T(8,128)(2,1)S(1)} %copy-done.1), channel_id=1, source_target_pairs={{0,2},{2,4},{4,6},{6,8},{8,10},{10,12},{12,14},{14,0},{1,3},{3,5},... | collective-permute-start | bytes 6291464 | tf_op jit(solution)/shard_map/ppermute | solution.py:65
  313.9 1.4 copy-start.2
  315.2 88.4 %collective-permute-start.1 = (bf16[4096,256]{1,0:T(8,128)(2,1)S(1)}, bf16[4096,256]{1,0:T(8,128)(2,1)S(1)}, u32[]{:S(2)}, u32[]{:S(2)}) collective-permute-start(bf16[4096,256]{1,0:T(8,128)(2,1)S(1)} %collective-permute-done), channel_id=1, source_target_pairs={{0,2},{2,4},{4,6},{6,8},{8,10},{10,12},{12,14},{14,0},{1,3},{3,5},... | collective-permute-start | bytes 6291464 | tf_op jit(solution)/shard_map/ppermute | solution.py:65
  403.6 1.3 copy-start.4
  405.0 95.6 %collective-permute-start.2 = (bf16[4096,256]{1,0:T(8,128)(2,1)S(1)}, bf16[4096,256]{1,0:T(8,128)(2,1)S(1)}, u32[]{:S(2)}, u32[]{:S(2)}) collective-permute-start(bf16[4096,256]{1,0:T(8,128)(2,1)S(1)} %collective-permute-done.1), channel_id=1, source_target_pairs={{0,2},{2,4},{4,6},{6,8},{8,10},{10,12},{12,14},{14,0},{1,3},{3,5},... | collective-permute-start | bytes 6291464 | tf_op jit(solution)/shard_map/ppermute | solution.py:65
  500.5 1.3 copy-start.6
  501.9 95.3 %collective-permute-start.3 = (bf16[4096,256]{1,0:T(8,128)(2,1)S(1)}, bf16[4096,256]{1,0:T(8,128)(2,1)S(1)}, u32[]{:S(2)}, u32[]{:S(2)}) collective-permute-start(bf16[4096,256]{1,0:T(8,128)(2,1)S(1)} %collective-permute-done.2), channel_id=1, source_target_pairs={{0,2},{2,4},{4,6},{6,8},{8,10},{10,12},{12,14},{14,0},{1,3},{3,5},... | collective-permute-start | bytes 6291464 | tf_op jit(solution)/shard_map/ppermute | solution.py:65
  597.2 1.3 copy-start.8
  598.5 76.4 %collective-permute-start.4 = (bf16[4096,256]{1,0:T(8,128)(2,1)S(1)}, bf16[4096,256]{1,0:T(8,128)(2,1)S(1)}, u32[]{:S(2)}, u32[]{:S(2)}) collective-permute-start(bf16[4096,256]{1,0:T(8,128)(2,1)S(1)} %collective-permute-done.3), channel_id=1, source_target_pairs={{0,2},{2,4},{4,6},{6,8},{8,10},{10,12},{12,14},{14,0},{1,3},{3,5},... | collective-permute-start | bytes 6291464 | tf_op jit(solution)/shard_map/ppermute | solution.py:65
  675.0 1.3 copy-start.10
  676.3 50.5 %collective-permute-start.5 = (bf16[4096,256]{1,0:T(8,128)(2,1)S(1)}, bf16[4096,256]{1,0:T(8,128)(2,1)}, u32[]{:S(2)}, u32[]{:S(2)}) collective-permute-start(bf16[4096,256]{1,0:T(8,128)(2,1)S(1)} %collective-permute-done.4), channel_id=1, source_target_pairs={{0,2},{2,4},{4,6},{6,8},{8,10},{10,12},{12,14},{14,0},{1,3},{3,5},... | collective-permute-start | bytes 6291464 | tf_op jit(solution)/shard_map/ppermute | solution.py:65
  726.8 49.2 %collective-permute-start.6 = (bf16[4096,256]{1,0:T(8,128)(2,1)}, bf16[4096,256]{1,0:T(8,128)(2,1)}, u32[]{:S(2)}, u32[]{:S(2)}) collective-permute-start(bf16[4096,256]{1,0:T(8,128)(2,1)} %collective-permute-done.5), channel_id=1, source_target_pairs={{0,2},{2,4},{4,6},{6,8},{8,10},{10,12},{12,14},{14,0},{1,3},{3,5},... | collective-permute-start | bytes 6291464 | tf_op jit(solution)/shard_map/ppermute | solution.py:65
  726.8 61.8 %copy-start.7 = (bf16[4096,256]{1,0:T(8,128)(2,1)S(1)}, bf16[4096,256]{1,0:T(8,128)(2,1)}, u32[]{:S(2)}) copy-start(bf16[4096,256]{1,0:T(8,128)(2,1)} %copy-done.6) | copy-start | bytes 6291460
  726.8 63.3 %copy-start.5 = (bf16[4096,256]{1,0:T(8,128)(2,1)S(1)}, bf16[4096,256]{1,0:T(8,128)(2,1)}, u32[]{:S(2)}) copy-start(bf16[4096,256]{1,0:T(8,128)(2,1)} %copy-done.4) | copy-start | bytes 6291460
  726.8 64.7 %copy-start.3 = (bf16[4096,256]{1,0:T(8,128)(2,1)S(1)}, bf16[4096,256]{1,0:T(8,128)(2,1)}, u32[]{:S(2)}) copy-start(bf16[4096,256]{1,0:T(8,128)(2,1)} %copy-done.2) | copy-start | bytes 6291460
  782.1 18.7 %copy-start.11 = (bf16[4096,256]{1,0:T(8,128)(2,1)S(1)}, bf16[4096,256]{1,0:T(8,128)(2,1)}, u32[]{:S(2)}) copy-start(bf16[4096,256]{1,0:T(8,128)(2,1)} %copy-done.10) | copy-start | bytes 6291460
  785.3 17.0 %copy-start.9 = (bf16[4096,256]{1,0:T(8,128)(2,1)S(1)}, bf16[4096,256]{1,0:T(8,128)(2,1)}, u32[]{:S(2)}) copy-start(bf16[4096,256]{1,0:T(8,128)(2,1)} %copy-done.8) | copy-start | bytes 6291460
  809.7 22.9 %copy-start.12 = (bf16[128,2048]{1,0:T(8,128)(2,1)S(1)}, bf16[128,2048]{1,0:T(8,128)(2,1)}, u32[]{:S(2)}) copy-start(bf16[128,2048]{1,0:T(8,128)(2,1)} %reduce-scatter.3.cloned.1.call-done) | copy-start | bytes 1572868
Sparse Core Ops, SparseCore 0:
  10.1 11.7 all-gather.7
  24.0 50.2 all-gather.13
  76.4 47.6 all-gather.11
  126.1 47.6 all-gather.9
  175.6 48.8 all-gather.15
  229.6 6.5 reduce-scatter.2
  239.7 10.2 all-gather.17
  252.2 364.0 all-gather.19
  826.4 6.2 reduce-scatter.4
